TPU v7x, 512 devices: a whole 4x4x16 slice. The times are simulated.
512 devices in a mesh: ep: 32 (over z, core), tp: 16 (over y, x).
Axes of the slice: x: 4, y: 4, z: 16, core: 2. Of those that a mesh axis runs over, the one named last changes fastest.
Arguments:
- conv_input: bfloat16 [1024, 65536], P('tp', 'ep'), may hold values from -6 to 6
- out_gate: bfloat16 [1024, 65536], P('tp', 'ep'), may hold values from -6 to 6
- in_gate: bfloat16 [1024, 65536], P('tp', 'ep'), may hold values from -6 to 6
- conv_taps: float32 [3, 1024], replicated, may hold values from -3.5 to 3.5
- mixer_proj: bfloat16 [1024, 2048], P(None, 'tp'), may hold values from -0.1875 to 0.1875
- token_rows: bfloat16 [8192, 2048], P('ep', 'tp'), may hold values from -4000 to 4000
- routes: int32 [8192, 2], P('ep'), may hold values from 0 to 31, as said below
- route_weights: float32 [8192, 2], P('ep'), may hold values from 0.3 to 1
- expert_gate: bfloat16 [32, 2048, 4096], P('ep', None, 'tp'), may hold values from -0.125 to 0.125
- expert_up: bfloat16 [32, 2048, 4096], P('ep', None, 'tp'), may hold values from -0.125 to 0.125
- expert_down: bfloat16 [32, 4096, 2048], P('ep', 'tp'), may hold values from -0.125 to 0.125
Outputs:
- mixed_out: bfloat16 [65536, 2048], P('ep', 'tp')
- expert_out: bfloat16 [8192, 2048], P('ep', 'tp')
Inputs may be any that keep to these rules, and one draw needn't show every extreme that they name: `routes`: in each aligned block of 256 rows, no expert is named more than 32 times and one expert, the same in every block, exactly 32 times; the two experts of a row differ.
All inputs are finite; a program needn't handle non-finite values.
Results may differ from a plain program's by a relative error of at most 0.015.
Values may be sent and summed in bfloat16 or wider, within the bound.
A program may use at most 64 MiB of HBM per device.

v0:
```python
import jax
import jax.numpy as jnp
from jax import lax
from jax.sharding import PartitionSpec as P

KERNEL = 3
EPSILON = 1e-06


def passed_along(value, axis, by):
    devices = lax.axis_size(axis)
    pairs = [(i, i + by) for i in range(devices) if 0 <= i + by < devices]
    return lax.ppermute(value, axis, pairs)


def split_up(value, dim, devices):
    before, after = (value.shape[:dim], value.shape[dim + 1 :])
    return jnp.moveaxis(value.reshape(*before, devices, -1, *after), dim, 0)


def sent_and_summed(value, axis, dim):
    blocks = split_up(value, dim, lax.axis_size(axis))
    arrived = lax.all_to_all(blocks, axis, split_axis=0, concat_axis=0, tiled=True)
    return arrived.astype(jnp.float32).sum(axis=0)


def slot_places(route_ids, capacity, experts):
    flat_ids = route_ids.reshape(-1)
    hit_table = (flat_ids[:, None] == jnp.arange(experts, dtype=jnp.int32)[None, :]).astype(
        jnp.int32
    )
    earlier = jnp.cumsum(hit_table, axis=0) - hit_table
    slot_rank = jnp.sum(earlier * hit_table, axis=1)
    return flat_ids * capacity + slot_rank


def body(
    conv_input,
    out_gate,
    in_gate,
    conv_taps,
    mixer_proj,
    token_rows,
    routes,
    route_weights,
    expert_gate,
    expert_up,
    expert_down,
):
    width_part = conv_input.shape[0]
    length = conv_input.shape[1]
    offset = lax.axis_index("tp") * width_part
    local_taps = lax.dynamic_slice_in_dim(conv_taps, offset, width_part, 1)
    z_rows = (conv_input.astype(jnp.float32) * in_gate.astype(jnp.float32)).astype(jnp.bfloat16)
    rim_rows = passed_along(z_rows[:, length - (KERNEL - 1) :], "ep", 1)
    longer = jnp.concatenate([rim_rows, z_rows], axis=1).astype(jnp.float32)
    conv_sum = jnp.zeros(z_rows.shape, jnp.float32)
    for lag_index in range(KERNEL):
        begin = KERNEL - 1 - lag_index
        conv_sum = conv_sum + local_taps[lag_index][:, None] * longer[:, begin : begin + length]
    gated = (out_gate.astype(jnp.float32) * conv_sum).astype(jnp.bfloat16)
    mixed_sum = lax.dot_general(
        lax.all_gather(gated, "tp", axis=0, tiled=True),
        mixer_proj,
        (((0,), (0,)), ((), ())),
        preferred_element_type=jnp.float32,
    )
    mixed_out = mixed_sum.astype(jnp.bfloat16)
    experts = lax.axis_size("ep")
    rows_b = token_rows.shape[0]
    cols_part = token_rows.shape[1]
    capacity = 4 * rows_b // experts
    slot_total = experts * capacity
    places = slot_places(routes, capacity, experts)
    sources = jnp.arange(2 * rows_b, dtype=jnp.int32) // 2
    gate_weight = expert_gate[0]
    up_weight = expert_up[0]
    down_weight = expert_down[0]
    feature_count = cols_part * lax.axis_size("tp")
    buffer = jnp.zeros((slot_total, cols_part), jnp.bfloat16).at[places].set(token_rows[sources])
    arrived = lax.all_to_all(
        buffer.reshape(experts, capacity, cols_part), "ep", split_axis=0, concat_axis=0, tiled=True
    )
    arrived = arrived.reshape(slot_total, cols_part)
    part_in = lax.all_gather(arrived, "tp", axis=1, tiled=True)
    gate_sum = jnp.dot(part_in, gate_weight, preferred_element_type=jnp.float32)
    up_sum = jnp.dot(part_in, up_weight, preferred_element_type=jnp.float32)
    squares = jnp.sum(jnp.square(part_in.astype(jnp.float32)), axis=1)
    row_scale = lax.rsqrt(squares / feature_count + EPSILON)[:, None]
    hidden = (jax.nn.silu(row_scale * gate_sum) * (row_scale * up_sum)).astype(jnp.bfloat16)
    summed = sent_and_summed(
        lax.dot_general(
            down_weight, hidden, (((0,), (1,)), ((), ())), preferred_element_type=jnp.float32
        ).astype(jnp.bfloat16),
        "tp",
        0,
    )
    expert_rows = summed.astype(jnp.bfloat16).reshape(cols_part, experts, capacity)
    returned = lax.all_to_all(expert_rows, "ep", split_axis=1, concat_axis=1, tiled=True).reshape(
        cols_part, slot_total
    )
    picked = returned[:, places].astype(jnp.float32).reshape(cols_part, rows_b, 2)
    combined = jnp.sum(picked * route_weights[None, :, :], axis=2)
    expert_out = combined.T.astype(jnp.bfloat16)
    return (mixed_out, expert_out)


def solution(mesh):
    return jax.shard_map(
        body,
        mesh=mesh,
        in_specs=(
            P("tp", "ep"),
            P("tp", "ep"),
            P("tp", "ep"),
            P(),
            P(None, "tp"),
            P("ep", "tp"),
            P("ep", None),
            P("ep", None),
            P("ep", None, "tp"),
            P("ep", None, "tp"),
            P("ep", "tp", None),
        ),
        out_specs=(P("ep", "tp"), P("ep", "tp")),
        check_vma=False,
    )
```

profile of v0, /device:TPU:1, one launch (start us, length us, event | category | flops | bytes accessed | tf_op | source)
XLA Modules:
  0.0 242.8 jit_solution(143505425020026601)
XLA Ops:
  7.2 0.0 copy-start
  7.2 0.0 all-gather.5.cloned.1.call-start
  7.2 0.9 copy.26
  8.1 0.1 eq.29
  8.3 0.1 eq.25
  8.4 0.7 broadcast_multiply_fusion
  9.1 1.2 reduce-window.6
  10.3 0.2 slice_reduce_fusion
  10.6 0.1 copy.25
  10.7 0.1 mul.101
  10.9 0.1 fusion.18
  11.0 4.9 %scatter_custom_fusion = bf16[1024,128]{1,0:T(8,128)(2,1)S(1)} fusion(s32[512]{0:T(512)S(1)} %bitcast.65, bf16[256,128]{1,0:T(8,128)(2,1)} %param.16, s32[1024]{0:T(1024)S(1)} %pad_clamp_fusion.1, bf16[]{:T(256)} %constant.39.clone.1), kind=kCustom, calls=%fused_computation.26 | custom fusion | bytes 262656 | tf_op jit(solution)/shard_map/scatter | solution.py:80
  15.9 38.9 %all_to_all.15 = bf16[32,32,128]{2,1,0:T(8,128)(2,1)} all-to-all(bf16[32,32,128]{2,1,0:T(8,128)(2,1)S(1)} %bitcast.63), channel_id=1, replica_groups=mesh['ep'=32,'tp'=16] {'ep'}, dimensions={0} | all-to-all | bytes 524288 | tf_op jit(solution)/shard_map/all_to_all | solution.py:81
  54.8 0.0 copy-start.3
  54.8 0.0 all-gather.5.cloned.1.call-update
  54.8 0.0 all-gather.3.cloned.1.call-start
  54.9 1.2 multiply_convert_fusion
  56.0 0.1 slice.40
  56.1 2.2 collective-permute-start
  58.4 0.8 constant_dynamic-slice_fusion
  59.1 0.1 collective-permute-done
  59.2 0.1 maximum_convert_fusion
  59.4 2.0 fusion.9
  61.4 0.0 all-gather.3.cloned.1.call-update
  61.4 55.6 %all-gather.5.cloned.1.call-done = bf16[1024,2048]{1,0:T(8,128)(2,1)} async-done(((bf16[1024,128]{1,0:T(8,128)(2,1)}), bf16[1024,2048]{1,0:T(8,128)(2,1)}) %all-gather.5.cloned.1.call-update) | async-done | bytes 4194320 | tf_op jit(solution)/shard_map/all_gather | solution.py:85
  117.1 0.0 copy-start.1
  117.1 3.2 %multiply_reduce_fusion = f32[1024]{0:T(1024)S(1)} fusion(bf16[1024,2048]{1,0:T(8,128)(2,1)} %all-gather.5.cloned.1.call-done), kind=kLoop, calls=%fused_computation.3 | loop fusion | flops 6290432 | bytes 4198400 | tf_op jit(solution)/shard_map/reduce_sum | solution.py:88
  120.3 0.0 copy-start.4
  120.3 0.0 copy-done.3
  120.3 0.2 copy-done.1
  120.5 2.3 convolution_multiply_fusion.1
  122.8 0.0 copy-done
  122.8 0.0 copy-done.4
  122.8 8.8 %convert_bitcast_fusion = bf16[128,16,8,128]{3,2,1,0:T(8,128)(2,1)} fusion(bf16[1,256,2048]{2,1,0:T(8,128)(2,1)S(1)} %copy-done, bf16[1024,2048]{1,0:T(8,128)(2,1)} %all-gather.5.cloned.1.call-done, bf16[1,2048,256]{2,1,0:T(8,128)(2,1)S(1)} %copy-done.4, f32[1024,256]{1,0:T(8,128)} %convolution_multiply_fusion.1, f32[1024]{0:T(1024)S(1)} %add_rsqrt_fusion), kind=kOutput, calls=%fused_computation.5 | convolution fusion | flops 2151415808 | bytes 11538432 | tf_op jit(solution)/shard_map/dot_general | solution.py:92
  131.6 3.3 %copy.35 = bf16[128,16,8,128]{3,2,0,1:T(8,128)(2,1)S(1)} copy(bf16[128,16,8,128]{3,2,1,0:T(8,128)(2,1)} %convert_bitcast_fusion) | data formatting | bytes 8388608 | tf_op jit(solution)/shard_map/reshape | solution.py:18
  134.9 58.8 %all_to_all.16 = bf16[16,128,1024]{1,2,0:T(8,128)(2,1)} all-to-all(bf16[16,128,1024]{1,2,0:T(8,128)(2,1)S(1)} %bitcast.59), channel_id=1, replica_groups=mesh['ep'=32,'tp'=16] {'tp'}, dimensions={0} | all-to-all | bytes 8388608 | tf_op jit(solution)/shard_map/all_to_all | solution.py:23
  193.7 0.0 copy-start.2
  193.7 0.0 copy-start.5
  193.7 3.9 %reduce_sum.44 = bf16[128,1024]{0,1:T(8,128)(2,1)} reduce(bf16[16,128,1024]{1,2,0:T(8,128)(2,1)} %all_to_all.16, bf16[]{:T(256)} %constant.39.clone.1), dimensions={0}, to_apply=%region_5.6 | reduce | flops 1966080 | bytes 4456450 | tf_op jit(solution)/shard_map/reduce_sum | solution.py:24
  197.6 13.7 %all-to-all-start.2 = ((bf16[128,32,32]{0,2,1:T(8,128)(2,1)}), bf16[128,32,32]{0,2,1:T(8,128)(2,1)S(1)}, u32[]{:S(2)}, u32[]{:S(2)}) async-start(bf16[128,32,32]{0,2,1:T(8,128)(2,1)} %bitcast.13), calls=%async_computation.2 | async-start | bytes 524288 | tf_op jit(solution)/shard_map/all_to_all | solution.py:99
  211.3 0.0 copy-done.2
  211.3 0.1 copy.30
  211.5 3.2 %all-gather.3.cloned.1.call-done = bf16[1024,2048]{1,0:T(8,128)(2,1)} async-done(((bf16[64,2048]{1,0:T(8,128)(2,1)}), bf16[1024,2048]{1,0:T(8,128)(2,1)}) %all-gather.3.cloned.1.call-update) | async-done | bytes 4194320 | tf_op jit(solution)/shard_map/all_gather | solution.py:63
  214.7 0.0 copy-done.5
  214.7 4.3 %convolution_convert_fusion = bf16[2048,128]{1,0:T(8,128)(2,1)} fusion(bf16[1024,2048]{1,0:T(8,128)(2,1)} %all-gather.3.cloned.1.call-done, bf16[1024,128]{1,0:T(8,128)(2,1)S(1)} %copy-done.5), kind=kOutput, calls=%fused_computation.6 | convolution fusion | flops 537133056 | bytes 4980736 | tf_op jit(solution)/shard_map/dot_general | solution.py:62
  219.0 14.6 %all-to-all-done.2 = bf16[128,32,32]{0,2,1:T(8,128)(2,1)S(1)} async-done(((bf16[128,32,32]{0,2,1:T(8,128)(2,1)}), bf16[128,32,32]{0,2,1:T(8,128)(2,1)S(1)}, u32[]{:S(2)}, u32[]{:S(2)}) %all-to-all-start.2) | async-done | bytes 262176 | tf_op jit(solution)/shard_map/all_to_all | solution.py:99
  233.6 1.3 gather_fusion
  234.9 1.0 multiply_reduce_fusion.1
  (10 shorter events, 0.1 us)
Async XLA Ops:
  7.2 115.7 %copy-start = (bf16[1,256,2048]{2,1,0:T(8,128)(2,1)S(1)}, bf16[1,256,2048]{2,1,0:T(8,128)(2,1)}, u32[]{:S(2)}) copy-start(bf16[1,256,2048]{2,1,0:T(8,128)(2,1)} %param.21) | copy-start | bytes 3145732
  7.2 109.9 %all-gather.5.cloned.1.call-start = ((), (), s32[]{:S(2)}) async-start(), calls=%async_computation.4 | async-start | bytes 4456448 | tf_op jit(solution)/shard_map/all_gather | solution.py:85
  54.8 65.5 %copy-start.3 = (bf16[1,2048,256]{2,1,0:T(8,128)(2,1)S(1)}, bf16[1,2048,256]{2,1,0:T(8,128)(2,1)}, u32[]{:S(2)}) copy-start(bf16[1,2048,256]{2,1,0:T(8,128)(2,1)} %param.19) | copy-start | bytes 3145732
  54.8 159.8 %all-gather.3.cloned.1.call-start = ((), (), s32[]{:S(2)}) async-start(), calls=%async_computation.3 | async-start | bytes 4456448 | tf_op jit(solution)/shard_map/all_gather | solution.py:63
  56.1 3.1 %collective-permute-start = (bf16[64,2]{1,0:T(8,128)(2,1)S(1)}, bf16[64,2]{1,0:T(8,128)(2,1)S(1)}, u32[]{:S(2)}, u32[]{:S(2)}) collective-permute-start(bf16[64,2]{1,0:T(8,128)(2,1)S(1)} %slice.40), channel_id=1, source_target_pairs={{0,16},{16,32},{32,48},{48,64},{64,80},{80,96},{96,112},{112,128},... | collective-permute-start | bytes 776 | tf_op jit(solution)/shard_map/ppermute | solution.py:13
  117.1 3.4 %copy-start.1 = (bf16[1024,2048]{1,0:T(8,128)(2,1)S(1)}, bf16[1024,2048]{1,0:T(8,128)(2,1)}, u32[]{:S(2)}) copy-start(bf16[1024,2048]{1,0:T(8,128)(2,1)} %all-gather.5.cloned.1.call-done) | copy-start | bytes 12582916
  120.3 2.5 %copy-start.4 = (bf16[1,2048,256]{2,1,0:T(8,128)(2,1)S(1)}, bf16[1,2048,256]{2,1,0:T(8,128)(2,1)}, u32[]{:S(2)}) copy-start(bf16[1,2048,256]{2,1,0:T(8,128)(2,1)} %param.20) | copy-start | bytes 3145732
  193.7 17.6 %copy-start.2 = (f32[256,2]{0,1:T(2,128)S(1)}, f32[256,2]{0,1:T(2,128)}, u32[]{:S(2)}) copy-start(f32[256,2]{0,1:T(2,128)} %param.18) | copy-start | bytes 6148
  193.7 21.0 %copy-start.5 = (bf16[1024,128]{1,0:T(8,128)(2,1)S(1)}, bf16[1024,128]{1,0:T(8,128)(2,1)}, u32[]{:S(2)}) copy-start(bf16[1024,128]{1,0:T(8,128)(2,1)} %param.15) | copy-start | bytes 786436
  197.6 35.9 %all-to-all-start.2 = ((bf16[128,32,32]{0,2,1:T(8,128)(2,1)}), bf16[128,32,32]{0,2,1:T(8,128)(2,1)S(1)}, u32[]{:S(2)}, u32[]{:S(2)}) async-start(bf16[128,32,32]{0,2,1:T(8,128)(2,1)} %bitcast.13), calls=%async_computation.2 | async-start | bytes 524288 | tf_op jit(solution)/shard_map/all_to_all | solution.py:99
Sparse Core Ops, SparseCore 0:
  54.9 62.0 all-gather.4
  120.6 93.9 all-gather.2
where the time goes:
time: 243 us
  blocking collectives  97.7 us (40%)
  waiting for transfers between devices  73.6 us (30%)
  starting transfers between devices  16 us (7%)
  matrix products  15.4 us (6%)
  between operations  14.2 us (6%)
  other arithmetic  13.6 us (6%)
  local copies, waits for them, and re-layouts  12.4 us (5%)
    all_to_all x1, blocking collectives, sent_and_summed(): lax.all_to_all(blocks, axis, split_axis=0, concat_axis=0, tiled=True)  58.8 us
    all_gather x1, waiting for transfers between devices, body(): part_in = lax.all_gather(arrived, 'tp', axis=1, tiled=True)  55.6 us
    all_to_all x1, blocking collectives, body(): lax.all_to_all(buffer.reshape(experts, capacity, cols_part), 'ep', split_...  38.9 us
    all_to_all x1, waiting for transfers between devices, body(): lax.all_to_all(expert_rows, 'ep', split_axis=1, concat_axis=1, tiled=True)  14.6 us
    all_to_all x1, starting transfers between devices, body(): lax.all_to_all(expert_rows, 'ep', split_axis=1, concat_axis=1, tiled=True)  13.7 us
    dot_general x1, matrix products, body(): lax.dot_general(down_weight, hidden, (((0,), (1,)), ((), ())), preferred_...  8.82 us
    scatter x1, local copies, waits for them, and re-layouts, body(): jnp.zeros((slot_total, cols_part), jnp.bfloat16).at[places]  4.9 us
  transfers between devices with their start and end apart: 4, of which 4 were waited for; matrix products, arithmetic and copies ran while one was open for 12% of the time, Pallas kernels for 0%

commit v1 on v0

--- a/solution.py
+++ b/solution.py
@@ -5,6 +5,28 @@
 
 KERNEL = 3
 EPSILON = 1e-06
+
+
+def in_order(blocks, dim):
+    shape = list(blocks.shape[1:])
+    shape[dim] *= blocks.shape[0]
+    return jnp.moveaxis(blocks, 0, dim).reshape(shape)
+
+
+def ring_gather(value, axis, dim):
+    size = lax.axis_size(axis)
+    pairs = [(i, (i + 1) % size) for i in range(size)]
+    back = [(b, a) for a, b in pairs]
+    lower, upper = ([], [])
+    for lap in range(size - 1):
+        if lap % 2 == 0:
+            lower.append(lax.ppermute(lower[-1] if lower else value, axis, pairs))
+        else:
+            upper.append(lax.ppermute(upper[-1] if upper else value, axis, back))
+    blocks = jnp.stack([*lower[::-1], value, *upper])
+    shift = lax.axis_index(axis) - len(lower)
+    blocks = blocks[(jnp.arange(size) - shift) % size]
+    return in_order(blocks, dim)
 
 
 def passed_along(value, axis, by):
@@ -82,7 +104,7 @@
         buffer.reshape(experts, capacity, cols_part), "ep", split_axis=0, concat_axis=0, tiled=True
     )
     arrived = arrived.reshape(slot_total, cols_part)
-    part_in = lax.all_gather(arrived, "tp", axis=1, tiled=True)
+    part_in = ring_gather(arrived, "tp", 1)
     gate_sum = jnp.dot(part_in, gate_weight, preferred_element_type=jnp.float32)
     up_sum = jnp.dot(part_in, up_weight, preferred_element_type=jnp.float32)
     squares = jnp.sum(jnp.square(part_in.astype(jnp.float32)), axis=1)

time: 243 us -> 305 us (1.26)
  starting transfers between devices: 16 us -> 84.6 us
  waiting for transfers between devices: 73.6 us -> 38.8 us
  local copies, waits for them, and re-layouts: 12.4 us -> 41.5 us
    ppermute x0 -> x15, starting transfers between devices: none -> 65.3 us  [the longest x7 48.8 us: ring_gather(): upper.append(lax.ppermute(upper[-1] if upper else value, axis, back))]
    all_gather x1 -> x0, waiting for transfers between devices: 55.6 us -> none  [body(): part_in = lax.all_gather(arrived, 'tp', axis=1, tiled=True)]
    ppermute x0 -> x15, waiting for transfers between devices: none -> 21 us  [the longest x8 16.8 us: ring_gather(): lower.append(lax.ppermute(lower[-1] if lower else value, axis, pairs))]
    unnamed x14 -> x29, local copies, waits for them, and re-layouts: 1.24 us -> 17.7 us
    transpose x0 -> x1, local copies, waits for them, and re-layouts: none -> 6.53 us  [in_order(): return jnp.moveaxis(blocks, 0, dim).reshape(shape)]
    gather x0 -> x1, local copies, waits for them, and re-layouts: none -> 5.27 us  [ring_gather(): blocks = blocks[(jnp.arange(size) - shift) % size]]
    all_gather x1, waiting for transfers between devices: 3.18 us -> 0.02 us  [body(): lax.all_gather(gated, 'tp', axis=0, tiled=True)]
    all_to_all x1, waiting for transfers between devices: 14.6 us -> 17.8 us  [body(): lax.all_to_all(expert_rows, 'ep', split_axis=1, concat_axis=1, tiled=True)]
  transfers between devices with their start and end apart: 4 -> 18, of which waited for: 4 -> 7; matrix products, arithmetic and copies ran while one was open for 12% -> 19% of each run, Pallas kernels for 0% -> 0%
where the time goes in v1:
time: 305 us; the launch traced here: 304 us
  blocking collectives  95.6 us (31%)
  starting transfers between devices  84.6 us (28%)
  local copies, waits for them, and re-layouts  41.5 us (14%)
  waiting for transfers between devices  38.8 us (13%)
  matrix products  15.5 us (5%)
  between operations  14.4 us (5%)
  other arithmetic  13.2 us (4%)
    all_to_all x1, blocking collectives, sent_and_summed(): lax.all_to_all(blocks, axis, split_axis=0, concat_axis=0, tiled=True)  56.9 us
    ppermute x7, starting transfers between devices, ring_gather(): upper.append(lax.ppermute(upper[-1] if upper else value, axis, back))  48.8 us
    all_to_all x1, blocking collectives, body(): lax.all_to_all(buffer.reshape(experts, capacity, cols_part), 'ep', split_...  38.8 us
    all_to_all x1, waiting for transfers between devices, body(): lax.all_to_all(expert_rows, 'ep', split_axis=1, concat_axis=1, tiled=True)  17.8 us
    unnamed x29, local copies, waits for them, and re-layouts  17.7 us
    ppermute x8, waiting for transfers between devices, ring_gather(): lower.append(lax.ppermute(lower[-1] if lower else value, axis, pairs))  16.8 us
    ppermute x8, starting transfers between devices, ring_gather(): lower.append(lax.ppermute(lower[-1] if lower else value, axis, pairs))  16.5 us
    all_to_all x1, starting transfers between devices, body(): lax.all_to_all(expert_rows, 'ep', split_axis=1, concat_axis=1, tiled=True)  14.9 us
  transfers between devices with their start and end apart: 18, of which 7 were waited for; matrix products, arithmetic and copies ran while one was open for 19% of the time, Pallas kernels for 0%

profile of v1, /device:TPU:1, one launch (start us, length us, event | category | flops | bytes accessed | tf_op | source)
XLA Modules:
  0.0 303.7 jit_solution(5204877694375823772)
XLA Ops:
  7.2 0.9 copy.26
  9.1 1.2 reduce-window.6
  11.0 4.9 %scatter_custom_fusion = bf16[1024,128]{1,0:T(8,128)(2,1)S(1)} fusion(s32[512]{0:T(512)S(1)} %bitcast.108, bf16[256,128]{1,0:T(8,128)(2,1)} %param.16, s32[1024]{0:T(1024)S(1)} %pad_clamp_fusion.2, bf16[]{:T(256)} %constant.55.clone.1), kind=kCustom, calls=%fused_computation.43 | custom fusion | bytes 262656 | tf_op jit(solution)/shard_map/scatter | solution.py:102
  15.9 38.8 %all_to_all.15 = bf16[32,32,128]{2,1,0:T(8,128)(2,1)S(1)} all-to-all(bf16[32,32,128]{2,1,0:T(8,128)(2,1)S(1)} %bitcast.106), channel_id=1, replica_groups=mesh['ep'=32,'tp'=16] {'ep'}, dimensions={0} | all-to-all | bytes 524288 | tf_op jit(solution)/shard_map/all_to_all | solution.py:103
  54.7 3.1 %collective-permute-start.1 = (bf16[1024,128]{1,0:T(8,128)(2,1)S(1)}, bf16[1024,128]{1,0:T(8,128)(2,1)S(1)}, u32[]{:S(2)}, u32[]{:S(2)}) collective-permute-start(bf16[1024,128]{1,0:T(8,128)(2,1)S(1)} %bitcast.103), channel_id=1, source_target_pairs={{0,1},{1,2},{2,3},{3,4},{4,5},{5,6},{6,7},{7,8},{8,9},{9,10},{10,1... | collective-permute-start | bytes 786440 | tf_op jit(solution)/shard_map/ppermute | solution.py:23
  57.8 9.6 %collective-permute-done.1 = bf16[1024,128]{1,0:T(8,128)(2,1)S(1)} collective-permute-done((bf16[1024,128]{1,0:T(8,128)(2,1)S(1)}, bf16[1024,128]{1,0:T(8,128)(2,1)S(1)}, u32[]{:S(2)}, u32[]{:S(2)}) %collective-permute-start.1) | collective-permute-done | bytes 262176 | tf_op jit(solution)/shard_map/ppermute | solution.py:23
  67.4 1.9 collective-permute-start.2
  69.3 6.7 %collective-permute-start.9 = (bf16[1024,128]{1,0:T(8,128)(2,1)S(1)}, bf16[1024,128]{1,0:T(8,128)(2,1)S(1)}, u32[]{:S(2)}, u32[]{:S(2)}) collective-permute-start(bf16[1024,128]{1,0:T(8,128)(2,1)S(1)} %bitcast.104), channel_id=1, source_target_pairs={{1,0},{2,1},{3,2},{4,3},{5,4},{6,5},{7,6},{8,7},{9,8},{10,9},{11,1... | collective-permute-start | bytes 786440 | tf_op jit(solution)/shard_map/ppermute | solution.py:25
  76.0 3.1 %collective-permute-done.2 = bf16[1024,128]{1,0:T(8,128)(2,1)S(1)} collective-permute-done((bf16[1024,128]{1,0:T(8,128)(2,1)S(1)}, bf16[1024,128]{1,0:T(8,128)(2,1)S(1)}, u32[]{:S(2)}, u32[]{:S(2)}) %collective-permute-start.2) | collective-permute-done | bytes 262176 | tf_op jit(solution)/shard_map/ppermute | solution.py:23
  79.1 1.9 collective-permute-start.3
  81.0 6.7 %collective-permute-start.10 = (bf16[1024,128]{1,0:T(8,128)(2,1)S(1)}, bf16[1024,128]{1,0:T(8,128)(2,1)S(1)}, u32[]{:S(2)}, u32[]{:S(2)}) collective-permute-start(bf16[1024,128]{1,0:T(8,128)(2,1)S(1)} %collective-permute-done.9), channel_id=1, source_target_pairs={{1,0},{2,1},{3,2},{4,3},{5,4},{6,5},{7,6},{8,7},{9,8},{10,9},{11,1... | collective-permute-start | bytes 786440 | tf_op jit(solution)/shard_map/ppermute | solution.py:25
  87.7 2.2 collective-permute-done.3
  90.0 1.9 collective-permute-start.4
  91.9 6.7 %collective-permute-start.11 = (bf16[1024,128]{1,0:T(8,128)(2,1)S(1)}, bf16[1024,128]{1,0:T(8,128)(2,1)S(1)}, u32[]{:S(2)}, u32[]{:S(2)}) collective-permute-start(bf16[1024,128]{1,0:T(8,128)(2,1)S(1)} %collective-permute-done.10), channel_id=1, source_target_pairs={{1,0},{2,1},{3,2},{4,3},{5,4},{6,5},{7,6},{8,7},{9,8},{10,9},{11,1... | collective-permute-start | bytes 786440 | tf_op jit(solution)/shard_map/ppermute | solution.py:25
  98.6 1.8 collective-permute-done.4
  100.4 1.9 collective-permute-start.5
  102.3 1.1 multiply_convert_fusion
  103.5 4.3 %collective-permute-start = (bf16[64,2]{1,0:T(8,128)(2,1)S(1)}, bf16[64,2]{1,0:T(8,128)(2,1)S(1)}, u32[]{:S(2)}, u32[]{:S(2)}) collective-permute-start(bf16[64,2]{1,0:T(8,128)(2,1)S(1)} %slice.42), channel_id=1, source_target_pairs={{0,16},{16,32},{32,48},{48,64},{64,80},{80,96},{96,112},{112,128},... | collective-permute-start | bytes 776 | tf_op jit(solution)/shard_map/ppermute | solution.py:35
  108.6 7.0 %collective-permute-start.12 = (bf16[1024,128]{1,0:T(8,128)(2,1)S(1)}, bf16[1024,128]{1,0:T(8,128)(2,1)}, u32[]{:S(2)}, u32[]{:S(2)}) collective-permute-start(bf16[1024,128]{1,0:T(8,128)(2,1)S(1)} %collective-permute-done.11), channel_id=1, source_target_pairs={{1,0},{2,1},{3,2},{4,3},{5,4},{6,5},{7,6},{8,7},{9,8},{10,9},{11,1... | collective-permute-start | bytes 786440 | tf_op jit(solution)/shard_map/ppermute | solution.py:25
  115.5 1.9 collective-permute-start.6
  117.5 2.5 collective-permute-done.12
  120.0 7.5 %collective-permute-start.13 = (bf16[1024,128]{1,0:T(8,128)(2,1)}, bf16[1024,128]{1,0:T(8,128)(2,1)}, u32[]{:S(2)}, u32[]{:S(2)}) collective-permute-start(bf16[1024,128]{1,0:T(8,128)(2,1)} %collective-permute-done.12), channel_id=1, source_target_pairs={{1,0},{2,1},{3,2},{4,3},{5,4},{6,5},{7,6},{8,7},{9,8},{10,9},{11,1... | collective-permute-start | bytes 786440 | tf_op jit(solution)/shard_map/ppermute | solution.py:25
  127.5 1.9 collective-permute-start.7
  129.6 1.8 collective-permute-done.13
  131.4 7.4 %collective-permute-start.14 = (bf16[1024,128]{1,0:T(8,128)(2,1)}, bf16[1024,128]{1,0:T(8,128)(2,1)S(1)}, u32[]{:S(2)}, u32[]{:S(2)}) collective-permute-start(bf16[1024,128]{1,0:T(8,128)(2,1)} %collective-permute-done.13), channel_id=1, source_target_pairs={{1,0},{2,1},{3,2},{4,3},{5,4},{6,5},{7,6},{8,7},{9,8},{10,9},{11,1... | collective-permute-start | bytes 786440 | tf_op jit(solution)/shard_map/ppermute | solution.py:25
  138.8 1.9 collective-permute-start.8
  140.8 2.0 fusion.9
  142.8 6.9 %collective-permute-start.15 = (bf16[1024,128]{1,0:T(8,128)(2,1)S(1)}, bf16[1024,128]{1,0:T(8,128)(2,1)S(1)}, u32[]{:S(2)}, u32[]{:S(2)}) collective-permute-start(bf16[1024,128]{1,0:T(8,128)(2,1)S(1)} %collective-permute-done.14), channel_id=1, source_target_pairs={{1,0},{2,1},{3,2},{4,3},{5,4},{6,5},{7,6},{8,7},{9,8},{10,9},{11,1... | collective-permute-start | bytes 786440 | tf_op jit(solution)/shard_map/ppermute | solution.py:25
  149.7 1.7 bitcast_dynamic-update-slice_fusion.15
  151.4 1.7 bitcast_dynamic-update-slice_fusion.14
  153.1 1.7 bitcast_dynamic-update-slice_fusion.13
  154.7 1.7 bitcast_dynamic-update-slice_fusion.12
  162.2 1.7 bitcast_dynamic-update-slice_fusion.3
  163.8 1.7 bitcast_dynamic-update-slice_fusion.2
  166.2 0.8 bitcast_dynamic-update-slice_fusion
  167.0 5.3 %gather_fusion = bf16[16,1024,128]{2,1,0:T(8,128)(2,1)} fusion(bf16[16,1024,128]{2,1,0:T(8,128)(2,1)} %bitcast_dynamic-update-slice_fusion, s32[1024]{0:T(1024)S(1)} %pad_clamp_fusion.1), kind=kCustom, calls=%fused_computation.1 | custom fusion | bytes 8388672 | tf_op jit(solution)/shard_map/gather | solution.py:28
  172.3 6.5 %copy.29 = bf16[1024,16,128]{0,2,1:T(8,128)(2,1)} copy(bf16[1024,16,128]{2,0,1:T(8,128)(2,1)} %bitcast.97) | data formatting | bytes 8388608 | tf_op jit(solution)/shard_map/transpose | solution.py:13
  178.8 3.2 %multiply_reduce_fusion = f32[1024]{0:T(1024)S(1)} fusion(bf16[16,1024,128]{2,1,0:T(8,128)(2,1)} %gather_fusion), kind=kLoop, calls=%fused_computation.4 | loop fusion | flops 6290432 | bytes 4198400 | tf_op jit(solution)/shard_map/reduce_sum | solution.py:110
  182.3 2.4 convolution_multiply_fusion.1
  184.6 8.8 %convert_bitcast_fusion = bf16[128,16,8,128]{3,2,1,0:T(8,128)(2,1)} fusion(bf16[1,256,2048]{2,1,0:T(8,128)(2,1)S(1)} %copy-done, bf16[1024,2048]{0,1:T(8,128)(2,1)} %bitcast.100, bf16[1,2048,256]{2,1,0:T(8,128)(2,1)S(1)} %copy-done.4, f32[1024,256]{1,0:T(8,128)} %convolution_multiply_fusion.1, f32[1024]{0:T(1024)S(1)} %add_rsqrt_fusion), kind=kOutput, calls=%fused_computation.6 | convolution fusion | flops 2151415808 | bytes 11538432 | tf_op jit(solution)/shard_map/dot_general | solution.py:114
  193.4 3.4 %copy.36 = bf16[128,16,8,128]{3,2,0,1:T(8,128)(2,1)S(1)} copy(bf16[128,16,8,128]{3,2,1,0:T(8,128)(2,1)} %convert_bitcast_fusion) | data formatting | bytes 8388608 | tf_op jit(solution)/shard_map/reshape | solution.py:40
  196.8 56.9 %all_to_all.16 = bf16[16,128,1024]{1,2,0:T(8,128)(2,1)} all-to-all(bf16[16,128,1024]{1,2,0:T(8,128)(2,1)S(1)} %bitcast.98), channel_id=1, replica_groups=mesh['ep'=32,'tp'=16] {'tp'}, dimensions={0} | all-to-all | bytes 8388608 | tf_op jit(solution)/shard_map/all_to_all | solution.py:45
  253.7 3.6 %reduce_sum.44 = bf16[128,1024]{0,1:T(8,128)(2,1)} reduce(bf16[16,128,1024]{1,2,0:T(8,128)(2,1)} %all_to_all.16, bf16[]{:T(256)} %constant.55.clone.1), dimensions={0}, to_apply=%region_5.6 | reduce | flops 1966080 | bytes 4456450 | tf_op jit(solution)/shard_map/reduce_sum | solution.py:46
  257.3 14.9 %all-to-all-start.2 = ((bf16[128,32,32]{0,2,1:T(8,128)(2,1)}), bf16[128,32,32]{0,2,1:T(8,128)(2,1)S(1)}, u32[]{:S(2)}, u32[]{:S(2)}) async-start(bf16[128,32,32]{0,2,1:T(8,128)(2,1)} %bitcast.32), calls=%async_computation.2 | async-start | bytes 524288 | tf_op jit(solution)/shard_map/all_to_all | solution.py:121
  272.4 4.3 %convolution_convert_fusion = bf16[2048,128]{1,0:T(8,128)(2,1)} fusion(bf16[1024,2048]{1,0:T(8,128)(2,1)} %all-gather.2.cloned.1.call-done, bf16[1024,128]{1,0:T(8,128)(2,1)S(1)} %copy-done.5), kind=kOutput, calls=%fused_computation.7 | convolution fusion | flops 537133056 | bytes 4980736 | tf_op jit(solution)/shard_map/dot_general | solution.py:84
  276.7 17.8 %all-to-all-done.2 = bf16[128,32,32]{0,2,1:T(8,128)(2,1)S(1)} async-done(((bf16[128,32,32]{0,2,1:T(8,128)(2,1)}), bf16[128,32,32]{0,2,1:T(8,128)(2,1)S(1)}, u32[]{:S(2)}, u32[]{:S(2)}) %all-to-all-start.2) | async-done | bytes 262176 | tf_op jit(solution)/shard_map/all_to_all | solution.py:121
  294.5 1.3 gather_fusion.1
  295.8 1.0 multiply_reduce_fusion.1
  (57 shorter events, 9.6 us)
Async XLA Ops:
  7.2 177.4 %copy-start = (bf16[1,256,2048]{2,1,0:T(8,128)(2,1)S(1)}, bf16[1,256,2048]{2,1,0:T(8,128)(2,1)}, u32[]{:S(2)}) copy-start(bf16[1,256,2048]{2,1,0:T(8,128)(2,1)} %param.21) | copy-start | bytes 3145732
  7.2 265.2 %all-gather.2.cloned.1.call-start = ((), (), s32[]{:S(2)}) async-start(), calls=%async_computation.3 | async-start | bytes 4456448 | tf_op jit(solution)/shard_map/all_gather | solution.py:85
  54.7 12.7 %collective-permute-start.1 = (bf16[1024,128]{1,0:T(8,128)(2,1)S(1)}, bf16[1024,128]{1,0:T(8,128)(2,1)S(1)}, u32[]{:S(2)}, u32[]{:S(2)}) collective-permute-start(bf16[1024,128]{1,0:T(8,128)(2,1)S(1)} %bitcast.103), channel_id=1, source_target_pairs={{0,1},{1,2},{2,3},{3,4},{4,5},{5,6},{6,7},{7,8},{8,9},{9,10},{10,1... | collective-permute-start | bytes 786440 | tf_op jit(solution)/shard_map/ppermute | solution.py:23
  67.4 11.7 %collective-permute-start.2 = (bf16[1024,128]{1,0:T(8,128)(2,1)S(1)}, bf16[1024,128]{1,0:T(8,128)(2,1)S(1)}, u32[]{:S(2)}, u32[]{:S(2)}) collective-permute-start(bf16[1024,128]{1,0:T(8,128)(2,1)S(1)} %collective-permute-done.1), channel_id=1, source_target_pairs={{0,1},{1,2},{2,3},{3,4},{4,5},{5,6},{6,7},{7,8},{8,9},{9,10},{10,1... | collective-permute-start | bytes 786440 | tf_op jit(solution)/shard_map/ppermute | solution.py:23
  69.3 11.7 %collective-permute-start.9 = (bf16[1024,128]{1,0:T(8,128)(2,1)S(1)}, bf16[1024,128]{1,0:T(8,128)(2,1)S(1)}, u32[]{:S(2)}, u32[]{:S(2)}) collective-permute-start(bf16[1024,128]{1,0:T(8,128)(2,1)S(1)} %bitcast.104), channel_id=1, source_target_pairs={{1,0},{2,1},{3,2},{4,3},{5,4},{6,5},{7,6},{8,7},{9,8},{10,9},{11,1... | collective-permute-start | bytes 786440 | tf_op jit(solution)/shard_map/ppermute | solution.py:25
  79.1 10.9 %collective-permute-start.3 = (bf16[1024,128]{1,0:T(8,128)(2,1)S(1)}, bf16[1024,128]{1,0:T(8,128)(2,1)S(1)}, u32[]{:S(2)}, u32[]{:S(2)}) collective-permute-start(bf16[1024,128]{1,0:T(8,128)(2,1)S(1)} %collective-permute-done.2), channel_id=1, source_target_pairs={{0,1},{1,2},{2,3},{3,4},{4,5},{5,6},{6,7},{7,8},{8,9},{9,10},{10,1... | collective-permute-start | bytes 786440 | tf_op jit(solution)/shard_map/ppermute | solution.py:23
  81.0 10.8 %collective-permute-start.10 = (bf16[1024,128]{1,0:T(8,128)(2,1)S(1)}, bf16[1024,128]{1,0:T(8,128)(2,1)S(1)}, u32[]{:S(2)}, u32[]{:S(2)}) collective-permute-start(bf16[1024,128]{1,0:T(8,128)(2,1)S(1)} %collective-permute-done.9), channel_id=1, source_target_pairs={{1,0},{2,1},{3,2},{4,3},{5,4},{6,5},{7,6},{8,7},{9,8},{10,9},{11,1... | collective-permute-start | bytes 786440 | tf_op jit(solution)/shard_map/ppermute | solution.py:25
  90.0 10.4 %collective-permute-start.4 = (bf16[1024,128]{1,0:T(8,128)(2,1)S(1)}, bf16[1024,128]{1,0:T(8,128)(2,1)S(1)}, u32[]{:S(2)}, u32[]{:S(2)}) collective-permute-start(bf16[1024,128]{1,0:T(8,128)(2,1)S(1)} %collective-permute-done.3), channel_id=1, source_target_pairs={{0,1},{1,2},{2,3},{3,4},{4,5},{5,6},{6,7},{7,8},{8,9},{9,10},{10,1... | collective-permute-start | bytes 786440 | tf_op jit(solution)/shard_map/ppermute | solution.py:23
  91.9 16.7 %collective-permute-start.11 = (bf16[1024,128]{1,0:T(8,128)(2,1)S(1)}, bf16[1024,128]{1,0:T(8,128)(2,1)S(1)}, u32[]{:S(2)}, u32[]{:S(2)}) collective-permute-start(bf16[1024,128]{1,0:T(8,128)(2,1)S(1)} %collective-permute-done.10), channel_id=1, source_target_pairs={{1,0},{2,1},{3,2},{4,3},{5,4},{6,5},{7,6},{8,7},{9,8},{10,9},{11,1... | collective-permute-start | bytes 786440 | tf_op jit(solution)/shard_map/ppermute | solution.py:25
  100.4 15.1 %collective-permute-start.5 = (bf16[1024,128]{1,0:T(8,128)(2,1)S(1)}, bf16[1024,128]{1,0:T(8,128)(2,1)}, u32[]{:S(2)}, u32[]{:S(2)}) collective-permute-start(bf16[1024,128]{1,0:T(8,128)(2,1)S(1)} %collective-permute-done.4), channel_id=1, source_target_pairs={{0,1},{1,2},{2,3},{3,4},{4,5},{5,6},{6,7},{7,8},{8,9},{9,10},{10,1... | collective-permute-start | bytes 786440 | tf_op jit(solution)/shard_map/ppermute | solution.py:23
  103.5 26.0 %collective-permute-start = (bf16[64,2]{1,0:T(8,128)(2,1)S(1)}, bf16[64,2]{1,0:T(8,128)(2,1)S(1)}, u32[]{:S(2)}, u32[]{:S(2)}) collective-permute-start(bf16[64,2]{1,0:T(8,128)(2,1)S(1)} %slice.42), channel_id=1, source_target_pairs={{0,16},{16,32},{32,48},{48,64},{64,80},{80,96},{96,112},{112,128},... | collective-permute-start | bytes 776 | tf_op jit(solution)/shard_map/ppermute | solution.py:35
  108.6 11.4 %collective-permute-start.12 = (bf16[1024,128]{1,0:T(8,128)(2,1)S(1)}, bf16[1024,128]{1,0:T(8,128)(2,1)}, u32[]{:S(2)}, u32[]{:S(2)}) collective-permute-start(bf16[1024,128]{1,0:T(8,128)(2,1)S(1)} %collective-permute-done.11), channel_id=1, source_target_pairs={{1,0},{2,1},{3,2},{4,3},{5,4},{6,5},{7,6},{8,7},{9,8},{10,9},{11,1... | collective-permute-start | bytes 786440 | tf_op jit(solution)/shard_map/ppermute | solution.py:25
  115.5 12.0 %collective-permute-start.6 = (bf16[1024,128]{1,0:T(8,128)(2,1)}, bf16[1024,128]{1,0:T(8,128)(2,1)}, u32[]{:S(2)}, u32[]{:S(2)}) collective-permute-start(bf16[1024,128]{1,0:T(8,128)(2,1)} %collective-permute-done.5), channel_id=1, source_target_pairs={{0,1},{1,2},{2,3},{3,4},{4,5},{5,6},{6,7},{7,8},{8,9},{9,10},{10,1... | collective-permute-start | bytes 786440 | tf_op jit(solution)/shard_map/ppermute | solution.py:23
  120.0 11.4 %collective-permute-start.13 = (bf16[1024,128]{1,0:T(8,128)(2,1)}, bf16[1024,128]{1,0:T(8,128)(2,1)}, u32[]{:S(2)}, u32[]{:S(2)}) collective-permute-start(bf16[1024,128]{1,0:T(8,128)(2,1)} %collective-permute-done.12), channel_id=1, source_target_pairs={{1,0},{2,1},{3,2},{4,3},{5,4},{6,5},{7,6},{8,7},{9,8},{10,9},{11,1... | collective-permute-start | bytes 786440 | tf_op jit(solution)/shard_map/ppermute | solution.py:25
  127.5 11.3 %collective-permute-start.7 = (bf16[1024,128]{1,0:T(8,128)(2,1)}, bf16[1024,128]{1,0:T(8,128)(2,1)}, u32[]{:S(2)}, u32[]{:S(2)}) collective-permute-start(bf16[1024,128]{1,0:T(8,128)(2,1)} %collective-permute-done.6), channel_id=1, source_target_pairs={{0,1},{1,2},{2,3},{3,4},{4,5},{5,6},{6,7},{7,8},{8,9},{9,10},{10,1... | collective-permute-start | bytes 786440 | tf_op jit(solution)/shard_map/ppermute | solution.py:23
  131.4 11.4 %collective-permute-start.14 = (bf16[1024,128]{1,0:T(8,128)(2,1)}, bf16[1024,128]{1,0:T(8,128)(2,1)S(1)}, u32[]{:S(2)}, u32[]{:S(2)}) collective-permute-start(bf16[1024,128]{1,0:T(8,128)(2,1)} %collective-permute-done.13), channel_id=1, source_target_pairs={{1,0},{2,1},{3,2},{4,3},{5,4},{6,5},{7,6},{8,7},{9,8},{10,9},{11,1... | collective-permute-start | bytes 786440 | tf_op jit(solution)/shard_map/ppermute | solution.py:25
  138.8 10.9 %collective-permute-start.8 = (bf16[1024,128]{1,0:T(8,128)(2,1)}, bf16[1024,128]{1,0:T(8,128)(2,1)}, u32[]{:S(2)}, u32[]{:S(2)}) collective-permute-start(bf16[1024,128]{1,0:T(8,128)(2,1)} %collective-permute-done.7), channel_id=1, source_target_pairs={{0,1},{1,2},{2,3},{3,4},{4,5},{5,6},{6,7},{7,8},{8,9},{9,10},{10,1... | collective-permute-start | bytes 786440 | tf_op jit(solution)/shard_map/ppermute | solution.py:23
  142.8 23.4 %collective-permute-start.15 = (bf16[1024,128]{1,0:T(8,128)(2,1)S(1)}, bf16[1024,128]{1,0:T(8,128)(2,1)S(1)}, u32[]{:S(2)}, u32[]{:S(2)}) collective-permute-start(bf16[1024,128]{1,0:T(8,128)(2,1)S(1)} %collective-permute-done.14), channel_id=1, source_target_pairs={{1,0},{2,1},{3,2},{4,3},{5,4},{6,5},{7,6},{8,7},{9,8},{10,9},{11,1... | collective-permute-start | bytes 786440 | tf_op jit(solution)/shard_map/ppermute | solution.py:25
  172.3 9.8 %copy-start.3 = (bf16[1,2048,256]{2,1,0:T(8,128)(2,1)S(1)}, bf16[1,2048,256]{2,1,0:T(8,128)(2,1)}, u32[]{:S(2)}) copy-start(bf16[1,2048,256]{2,1,0:T(8,128)(2,1)} %param.19) | copy-start | bytes 3145732
  178.8 3.4 %copy-start.1 = (bf16[1024,16,128]{0,2,1:T(8,128)(2,1)S(1)}, bf16[1024,16,128]{0,2,1:T(8,128)(2,1)}, u32[]{:S(2)}) copy-start(bf16[1024,16,128]{0,2,1:T(8,128)(2,1)} %copy.29) | copy-start | bytes 12582916
  182.2 2.4 copy-start.4
  253.7 18.5 %copy-start.2 = (f32[256,2]{0,1:T(2,128)S(1)}, f32[256,2]{0,1:T(2,128)}, u32[]{:S(2)}) copy-start(f32[256,2]{0,1:T(2,128)} %param.18) | copy-start | bytes 6148
  253.7 18.7 %copy-start.5 = (bf16[1024,128]{1,0:T(8,128)(2,1)S(1)}, bf16[1024,128]{1,0:T(8,128)(2,1)}, u32[]{:S(2)}) copy-start(bf16[1024,128]{1,0:T(8,128)(2,1)} %param.15) | copy-start | bytes 786436
  257.3 37.2 %all-to-all-start.2 = ((bf16[128,32,32]{0,2,1:T(8,128)(2,1)}), bf16[128,32,32]{0,2,1:T(8,128)(2,1)S(1)}, u32[]{:S(2)}, u32[]{:S(2)}) async-start(bf16[128,32,32]{0,2,1:T(8,128)(2,1)} %bitcast.32), calls=%async_computation.2 | async-start | bytes 524288 | tf_op jit(solution)/shard_map/all_to_all | solution.py:121
Sparse Core Ops, SparseCore 0:
  142.9 75.0 all-gather.1
